TPU v7x, 32 devices: a whole 2x2x4 slice. The times are simulated.
32 devices in a mesh: tp: 8 (over z, x), dp: 4 (over y, core).
Axes of the slice: x: 2, y: 2, z: 4, core: 2. Of those that a mesh axis runs over, the one named last changes fastest.
Arguments:
- stream_in: bfloat16 [256, 4096], P('tp', 'dp'), may hold values from -21 to 21
- hidden_state: float32 [2, 256, 4096], P(None, 'dp', 'tp'), may hold values from -6 to 6
- convolution_window_state: bfloat16 [2, 256, 3, 4096], P(None, 'dp', None, 'tp'), may hold values from -6 to 6
- norm_gain: float32 [2, 4096], P(None, 'dp'), may hold values from 0.1 to 1.9
- path_weight: bfloat16 [2, 4096, 4096], P(None, 'dp', 'tp'), may hold values from -0.09375 to 0.09375
- output_gate_weight: bfloat16 [2, 4096, 4096], P(None, 'dp', 'tp'), may hold values from -0.09375 to 0.09375
- conv_taps: float32 [2, 4, 4096], P(None, None, 'tp'), may hold values from -3 to 3
- recur_map: float32 [2, 64, 64, 64], P(None, 'tp'), may hold values from -0.75 to 0.75
- input_map: float32 [2, 64, 64, 64], P(None, 'tp'), may hold values from -0.75 to 0.75
- decay_logit: float32 [2, 4096], P(None, 'tp'), may hold values from 1 to 6
- out_weight: bfloat16 [2, 4096, 4096], P(None, 'tp', 'dp'), may hold values from -0.09375 to 0.09375
Outputs:
- stream_out: bfloat16 [256, 4096], P('tp', 'dp')
- hidden_next: float32 [2, 256, 4096], P(None, 'dp', 'tp')
- conv_next: bfloat16 [2, 256, 3, 4096], P(None, 'dp', None, 'tp')
All inputs are finite; a program needn't handle non-finite values.
Results may differ from a plain program's by a relative error of at most 0.019.
Values may be sent and summed in bfloat16 or wider, within the bound.
A program may use at most 64 MiB of HBM per device.

v0:
```python
import jax
import jax.numpy as jnp
from jax import lax
from jax.sharding import PartitionSpec as P

D = 4096
TAPS = 4


EPS = 1e-06


def scaled(rows, gain):
    rowsf = rows.astype(jnp.float32)
    sumsq = lax.psum(jnp.sum(rowsf * rowsf, axis=1), "dp")
    return (rowsf * lax.rsqrt(sumsq / D + EPS)[:, None] * gain[None, :]).astype(jnp.bfloat16)


def shard_inputs(normed, path_w, gate_branch_matrix):
    return jnp.concatenate(
        [
            jnp.dot(normed, path_w, preferred_element_type=jnp.float32),
            jnp.dot(normed, gate_branch_matrix, preferred_element_type=jnp.float32),
        ],
        axis=1,
    )


def recur_tail(partial_value, hidden, buffer, taps, recur_w, input_matrix, logit, out_w):
    width = partial_value.shape[1] // 2
    summed = lax.psum_scatter(
        partial_value.astype(jnp.bfloat16), "dp", scatter_dimension=0, tiled=True
    ).astype(jnp.float32)
    zpath = summed[:, :width].astype(jnp.bfloat16)
    zgate = summed[:, width:].astype(jnp.bfloat16)
    batch = zpath.shape[0]
    conv = zpath.astype(jnp.float32) * taps[TAPS - 1][None, :]
    for j in range(TAPS - 1):
        conv = conv + buffer[:, j].astype(jnp.float32) * taps[j][None, :]
    new_buffer = jnp.concatenate([buffer[:, 1:], zpath[:, None, :]], axis=1)
    cblocks = conv.reshape(batch, recur_w.shape[0], recur_w.shape[1])
    rgate = jax.nn.sigmoid(
        jnp.einsum("bnc,ncd->bnd", cblocks, recur_w, precision=lax.Precision.HIGHEST).reshape(
            batch, width
        )
    )
    igate = jax.nn.sigmoid(
        jnp.einsum("bnc,ncd->bnd", cblocks, input_matrix, precision=lax.Precision.HIGHEST).reshape(
            batch, width
        )
    )
    loga = 8.0 * rgate * jax.nn.log_sigmoid(logit)[None, :]
    new_hidden = jnp.exp(loga) * hidden + jnp.sqrt(-jnp.expm1(2.0 * loga)) * (igate * conv)
    mixed = (new_hidden * jax.nn.gelu(zgate.astype(jnp.float32))).astype(jnp.bfloat16)
    update = jnp.dot(
        lax.all_gather(mixed, "dp", axis=0, tiled=True), out_w, preferred_element_type=jnp.float32
    )
    return (update, new_hidden, new_buffer)


def per_device(
    stream_in,
    hidden_state,
    convolution_window_state,
    norm_gain,
    path_weight,
    output_gate_weight,
    conv_taps,
    recur_map,
    input_map,
    decay_logit,
    out_weight,
):
    stream = stream_in
    own_rows = stream.shape[0]
    whole_rows = lax.all_gather(stream, "tp", axis=0, tiled=True)
    partial_value = shard_inputs(
        scaled(whole_rows, norm_gain[0]), path_weight[0], output_gate_weight[0]
    )
    update, hidden_first, buffer_first = recur_tail(
        partial_value,
        hidden_state[0],
        convolution_window_state[0],
        conv_taps[0],
        recur_map[0],
        input_map[0],
        decay_logit[0],
        out_weight[0],
    )
    whole_rows = (
        whole_rows.astype(jnp.float32)
        + lax.psum(update.astype(jnp.bfloat16), "tp").astype(jnp.float32)
    ).astype(jnp.bfloat16)
    stream = lax.dynamic_slice_in_dim(whole_rows, lax.axis_index("tp") * own_rows, own_rows, 0)
    partial_value = shard_inputs(
        scaled(whole_rows, norm_gain[1]), path_weight[1], output_gate_weight[1]
    )
    update, hidden_second, buffer_second = recur_tail(
        partial_value,
        hidden_state[1],
        convolution_window_state[1],
        conv_taps[1],
        recur_map[1],
        input_map[1],
        decay_logit[1],
        out_weight[1],
    )
    stream = (
        stream.astype(jnp.float32)
        + lax.psum_scatter(
            update.astype(jnp.bfloat16), "tp", scatter_dimension=0, tiled=True
        ).astype(jnp.float32)
    ).astype(jnp.bfloat16)
    return (
        stream,
        jnp.stack([hidden_first, hidden_second]),
        jnp.stack([buffer_first, buffer_second]),
    )


def solution(mesh):
    placed = (
        P("tp", "dp"),
        P(None, "dp", "tp"),
        P(None, "dp", None, "tp"),
        P(None, "dp"),
        P(None, "dp", "tp"),
        P(None, "dp", "tp"),
        P(None, None, "tp"),
        P(None, "tp", None, None),
        P(None, "tp", None, None),
        P(None, "tp"),
        P(None, "tp", "dp"),
    )
    return jax.shard_map(
        per_device,
        mesh=mesh,
        in_specs=placed,
        out_specs=(P("tp", "dp"), P(None, "dp", "tp"), P(None, "dp", None, "tp")),
        check_vma=False,
    )
```

profile of v0, /device:TPU:0, one launch (start us, length us, event | category | flops | bytes accessed | tf_op | source)
XLA Modules:
  0.0 273.3 jit_solution(6701813631112867698)
XLA Ops:
  7.2 33.3 %all_gather.9 = bf16[256,1024]{1,0:T(8,128)(2,1)S(1)} all-gather(bf16[32,1024]{1,0:T(8,128)(2,1)} %param.11), channel_id=1, replica_groups=mesh['tp'=8,'dp'=4] {'tp'}, dimensions={0}, use_global_device_ids=true | all-gather | bytes 589824 | tf_op jit(solution)/shard_map/all_gather | solution.py:76
  40.6 5.7 %psum.21 = f32[256]{0:T(256)S(1)} all-reduce(f32[256]{0:T(256)S(1)} %fusion.19), channel_id=1, replica_groups=mesh['tp'=8,'dp'=4] {'dp'}, use_global_device_ids=true, to_apply=%region_1.0 | all-reduce | flops 256 | bytes 2048 | tf_op jit(solution)/shard_map/psum | solution.py:15
  46.3 0.9 fusion.81
  47.2 1.7 convolution_convert_fusion.5
  49.5 0.9 pad_maximum_fusion
  50.5 22.9 %reduce-scatter.4.cloned.1.call-done = bf16[64,1024]{1,0:T(8,128)(2,1)} async-done(((bf16[256,1024]{1,0:T(8,128)(2,1)}), bf16[64,1024]{1,0:T(8,128)(2,1)}) %reduce-scatter.4.cloned.1.call-update) | async-done | bytes 131088 | tf_op jit(solution)/shard_map/reduce_scatter | solution.py:31
  73.4 0.9 fusion.68
  75.2 1.4 fusion.11
  77.1 5.8 %all_gather.10 = bf16[256,512]{1,0:T(8,128)(2,1)S(1)} all-gather(bf16[64,512]{1,0:T(8,128)(2,1)S(1)} %get-tuple-element.7), channel_id=1, replica_groups=mesh['tp'=8,'dp'=4] {'dp'}, dimensions={0}, use_global_device_ids=true | all-gather | bytes 327680 | tf_op jit(solution)/shard_map/all_gather | solution.py:56
  82.8 2.5 convolution_convert_fusion.1
  85.4 72.8 %all-reduce.2.cloned.1.call-done = bf16[256,1024]{1,0:T(8,128)(2,1)} async-done(((bf16[256,1024]{1,0:T(8,128)(2,1)}), bf16[256,1024]{1,0:T(8,128)(2,1)}) %all-reduce.2.cloned.1.call-update) | async-done | bytes 524304 | tf_op jit(solution)/shard_map/psum | solution.py:92
  158.2 1.3 fusion.16
  159.5 5.7 %psum.23 = f32[256]{0:T(256)S(1)} all-reduce(f32[256]{0:T(256)S(1)} %get-tuple-element.5), channel_id=1, replica_groups=mesh['tp'=8,'dp'=4] {'dp'}, use_global_device_ids=true, to_apply=%region_5.6 | all-reduce | flops 256 | bytes 2048 | tf_op jit(solution)/shard_map/psum | solution.py:15
  165.2 1.7 convolution_convert_fusion.3
  166.9 1.7 convolution_convert_fusion.2
  168.6 0.9 pad_maximum_fusion.1
  169.5 21.2 %reduce-scatter.6.cloned.1.call-done = bf16[64,1024]{1,0:T(8,128)(2,1)} async-done(((bf16[256,1024]{1,0:T(8,128)(2,1)}), bf16[64,1024]{1,0:T(8,128)(2,1)}) %reduce-scatter.6.cloned.1.call-update) | async-done | bytes 131088 | tf_op jit(solution)/shard_map/reduce_scatter | solution.py:31
  190.7 0.9 fusion.65
  192.2 1.4 fusion.3
  194.3 5.8 %all_gather.11 = bf16[256,512]{1,0:T(8,128)(2,1)S(1)} all-gather(bf16[64,512]{1,0:T(8,128)(2,1)S(1)} %get-tuple-element.3), channel_id=1, replica_groups=mesh['tp'=8,'dp'=4] {'dp'}, dimensions={0}, use_global_device_ids=true | all-gather | bytes 327680 | tf_op jit(solution)/shard_map/all_gather | solution.py:56
  200.1 2.5 convolution_convert_fusion
  203.5 0.8 pad_maximum_fusion.2
  204.2 61.1 %reduce-scatter.8.cloned.1.call-done = bf16[32,1024]{1,0:T(8,128)(2,1)} async-done(((bf16[256,1024]{1,0:T(8,128)(2,1)}), bf16[32,1024]{1,0:T(8,128)(2,1)}) %reduce-scatter.8.cloned.1.call-update) | async-done | bytes 65552 | tf_op jit(solution)/shard_map/reduce_scatter | solution.py:110
  265.3 1.5 add_convert_fusion
  (52 shorter events, 4.4 us)
Async XLA Ops:
  7.2 66.3 %reduce-scatter.4.cloned.1.call-start = ((), (), s32[]{:S(2)}) async-start(), calls=%async_computation.3 | async-start | bytes 655360 | tf_op jit(solution)/shard_map/reduce_scatter | solution.py:31
  46.3 2.6 copy-start.6
  48.9 1.5 copy-start.5
  48.9 1.5 copy-start.4
  48.9 1.5 copy-start
  49.4 25.0 %copy-start.7 = (f32[2,8,64,64]{3,2,1,0:T(8,128)S(1)}, f32[2,8,64,64]{3,2,1,0:T(8,128)}, u32[]{:S(2)}) copy-start(f32[2,8,64,64]{3,2,1,0:T(8,128)} %param.18) | copy-start | bytes 786436
  50.3 107.9 %all-reduce.2.cloned.1.call-start = ((), (), s32[]{:S(2)}) async-start(), calls=%async_computation.4 | async-start | bytes 1048576 | tf_op jit(solution)/shard_map/psum | solution.py:92
  74.4 2.4 copy-start.1
  74.4 2.4 copy-start.3
  85.3 105.4 %reduce-scatter.6.cloned.1.call-start = ((), (), s32[]{:S(2)}) async-start(), calls=%async_computation.5 | async-start | bytes 655360 | tf_op jit(solution)/shard_map/reduce_scatter | solution.py:31
  169.5 95.8 %reduce-scatter.8.cloned.1.call-start = ((), (), s32[]{:S(2)}) async-start(), calls=%async_computation.6 | async-start | bytes 589824 | tf_op jit(solution)/shard_map/reduce_scatter | solution.py:110
  191.7 2.4 copy-start.2
Sparse Core Ops, SparseCore 0:
  50.5 22.9 reduce-scatter.3
  85.5 72.6 all-reduce.1
  169.6 21.0 reduce-scatter.5
  202.7 62.5 reduce-scatter.7
where the time goes:
time: 274 us; the launch traced here: 273 us
  waiting for transfers between devices  178 us (65%)
  blocking collectives  56.1 us (20%)
  matrix products  14.2 us (5%)
  between operations  14 us (5%)
  other arithmetic  8.41 us (3%)
    psum x1, waiting for transfers between devices, per_device(): lax.psum(update.astype(jnp.bfloat16), 'tp').astype(jnp.float32)  72.8 us
    reduce_scatter x1, waiting for transfers between devices, per_device(): lax.psum_scatter(update.astype(jnp.bfloat16), 'tp', scatter_dimension=0,...  61.1 us
    reduce_scatter x2, waiting for transfers between devices, recur_tail(): lax.psum_scatter(partial_value.astype(jnp.bfloat16), 'dp', scatter_dimens...  44.1 us
    all_gather x1, blocking collectives, per_device(): whole_rows = lax.all_gather(stream, 'tp', axis=0, tiled=True)  33.3 us
    all_gather x2, blocking collectives, recur_tail(): lax.all_gather(mixed, 'dp', axis=0, tiled=True)  11.6 us
    psum x2, blocking collectives, scaled(): sumsq = lax.psum(jnp.sum(rowsf * rowsf, axis=1), 'dp')  11.3 us
  transfers between devices with their start and end apart: 4, of which 4 were waited for; matrix products, arithmetic and copies ran while one was open for 1% of the time, Pallas kernels for 0%

commit v1 on v0

v1 whole, which is shorter than its diff:
```python
import functools

import jax
import jax.numpy as jnp
from jax import lax
from jax.experimental import pallas as pl
from jax.experimental.pallas import tpu as pltpu
from jax.sharding import PartitionSpec as P

EPS = 1e-06
MESH = pl.DeviceIdType.MESH
LANES = 128
F32 = jnp.float32
BF16 = jnp.bfloat16


def partner(index, step, count):
    if count & (count - 1):
        raise ValueError(count)
    out = index
    bit = 1
    while bit < count:
        if step & bit:
            out = out + bit - 2 * bit * ((index // bit) % 2)
        bit *= 2
    return out


def pack_col(col):
    high = col.astype(BF16).astype(F32)
    low = col - high
    lane = lax.broadcasted_iota(jnp.int32, (col.shape[0], LANES), 1)
    return jnp.where(lane < LANES // 2, high, low).astype(BF16)


def unpack_col(lanes):
    return lanes[:, 0:1] + lanes[:, LANES // 2 : LANES // 2 + 1]


def step_kernel(
    sizes,
    stream, hidden_hbm, convpart_hbm, gain, path_hbm, gate_hbm, taps, rmap_hbm, imap_hbm, logit, outw_hbm,
    stream_out, hidden_out, zpath_out,
    xg, part, core_in, y_send, y_in, mix, upd, x_in, z_send, z_in,
    wpath, wgate, wout, hid, convp, rmap, imap, diag,
    load_sem, load_small, ag_s, ag_r, fw_s, fw_r, b1_s, b1_r, b2_s, b2_r,
    c1_s, c1_r, c2_s, c2_r, d1_s, d1_r, d2_s, d2_r,
):
    layers, nz, nx, ny, nc, model = sizes
    tp = lax.axis_index("tp")
    dp = lax.axis_index("dp")
    z, x = tp // nx, tp % nx
    y, c = dp // nc, dp % nc
    rows, cols = stream.shape
    chans = wpath.shape[2]
    per_z = mix.shape[1] // nz
    chunk = mix.shape[2]

    def on_tp(zz, xx):
        return {"tp": zz * nx + xx, "dp": dp}

    def on_dp(yy, cc):
        return {"tp": tp, "dp": yy * nc + cc}

    loads = {}

    def load(name, layer, src, dst, sem):
        copy = pltpu.make_async_copy(src.at[layer], dst.at[layer], sem)
        copy.start()
        loads[name, layer] = copy

    peers = (
        [on_tp(partner(z, k, nz), x) for k in range(1, nz)]
        + [on_tp(z, partner(x, k, nx)) for k in range(1, nx)]
        + [on_dp(partner(y, k, ny), c) for k in range(1, ny)]
        + [on_dp(y, partner(c, k, nc)) for k in range(1, nc)]
    )
    barrier = pltpu.get_barrier_semaphore()
    for peer in peers:
        pl.semaphore_signal(barrier, inc=1, device_id=peer, device_id_type=MESH)
    xg[0, tp] = stream[...]
    load("path", 0, path_hbm, wpath, load_sem.at[0, 0])
    load("gate", 0, gate_hbm, wgate, load_sem.at[0, 1])
    for layer in range(layers):
        load("rmap", layer, rmap_hbm, rmap, load_small.at[layer, 0])
        load("imap", layer, imap_hbm, imap, load_small.at[layer, 1])
    pl.semaphore_wait(barrier, len(peers))

    sends = []

    def send(src, dst, ssem, rsem, peer):
        copy = pltpu.make_async_remote_copy(
            src_ref=src, dst_ref=dst, send_sem=ssem, recv_sem=rsem, device_id=peer, device_id_type=MESH
        )
        copy.start()
        sends.append(copy)

    def arrived(dst, ssem, rsem, peer):
        pltpu.make_async_remote_copy(
            src_ref=dst, dst_ref=dst, send_sem=ssem, recv_sem=rsem, device_id=peer, device_id_type=MESH
        ).wait_recv()

    def gather_start(layer):
        own = xg.at[layer, tp]
        source = stream if layer == 0 else own
        for k in range(1, nz):
            send(source, own, ag_s.at[layer, k], ag_r.at[layer, k], on_tp(partner(z, k, nz), x))
        for j in range(1, nx):
            send(source, own, fw_s.at[layer, 0, j], fw_r.at[layer, 0, j], on_tp(z, partner(x, j, nx)))

    def project(layer, zz):
        block = xg[layer, pl.ds(zz * nx, nx)].reshape(nx * rows, cols).astype(F32)
        scaled = (block * gain[layer : layer + 1, :]).astype(BF16)
        square = jnp.sum(block * block, axis=1, keepdims=True)
        shape = (per_z, chunk)
        here = pl.ds(zz * per_z, per_z)
        part[layer, here, :, 0:chans] = (
            jnp.dot(scaled, wpath[layer], preferred_element_type=F32).astype(BF16).reshape(*shape, chans)
        )
        part[layer, here, :, chans : 2 * chans] = (
            jnp.dot(scaled, wgate[layer], preferred_element_type=F32).astype(BF16).reshape(*shape, chans)
        )
        part[layer, here, :, 2 * chans :] = pack_col(square).reshape(*shape, LANES)

    def gather_and_project(layer):
        for k in range(nz):
            zz = partner(z, k, nz)
            if k:
                own = xg.at[layer, zz * nx + x]
                arrived(own, ag_s.at[layer, k], ag_r.at[layer, k], on_tp(zz, x))
                for j in range(1, nx):
                    send(own, own, fw_s.at[layer, k, j], fw_r.at[layer, k, j], on_tp(z, partner(x, j, nx)))
            if k == 0:
                loads["path", layer].wait()
                loads["gate", layer].wait()
            else:
                finish_block(layer, k - 1)
        finish_block(layer, nz - 1)

    def finish_block(layer, k):
        zz = partner(z, k, nz)
        for j in range(1, nx):
            xx = partner(x, j, nx)
            arrived(xg.at[layer, zz * nx + xx], fw_s.at[layer, k, j], fw_r.at[layer, k, j], on_tp(z, xx))
        project(layer, zz)

    def reduce_rows(layer):
        order = list(range(1, ny)) + [0]
        for k in order:
            yy = partner(y, k, ny)
            for j in range(1, nc):
                cc = partner(c, j, nc)
                send(
                    part.at[layer, yy * nc + cc], core_in.at[layer, j, k],
                    b1_s.at[layer, j, k], b1_r.at[layer, j, k], on_dp(y, cc),
                )
        total = None
        for k in order:
            yy = partner(y, k, ny)
            both = part[layer, yy * nc + c].astype(F32)
            extra = None
            for j in range(1, nc):
                arrived(
                    core_in.at[layer, j, k], b1_s.at[layer, j, k], b1_r.at[layer, j, k],
                    on_dp(y, partner(c, j, nc)),
                )
                both = both + core_in[layer, j, k].astype(F32)
            if k:
                y_send[layer, k, :, 0 : 2 * chans] = both[:, : 2 * chans].astype(BF16)
                y_send[layer, k, :, 2 * chans :] = pack_col(unpack_col(both[:, 2 * chans :]))
                send(y_send.at[layer, k], y_in.at[layer, k], b2_s.at[layer, k], b2_r.at[layer, k], on_dp(yy, c))
            else:
                total = both
        for k in range(1, ny):
            arrived(y_in.at[layer, k], b2_s.at[layer, k], b2_r.at[layer, k], on_dp(partner(y, k, ny), c))
            total = total + y_in[layer, k].astype(F32)
        return total

    def recur(layer, total):
        loads["hidden", layer].wait()
        loads["convpart", layer].wait()
        scale = lax.rsqrt(unpack_col(total[:, 2 * chans :]) / model + EPS)
        zpath = (total[:, :chans] * scale).astype(BF16)
        zgate = (total[:, chans : 2 * chans] * scale).astype(BF16).astype(F32)
        zpath_out[layer] = zpath
        last = taps.shape[1] - 1
        conv = convp[layer] + zpath.astype(F32) * taps[layer, last : last + 1, :]
        keep = jax.nn.log_sigmoid(logit[layer : layer + 1, :]) * 8.0
        gated = 0.5 * zgate * (1.0 + jnp.tanh(0.7978845608028654 * (zgate + 0.044715 * zgate * zgate * zgate)))
        wide = diag.shape[2]
        for p in range(diag.shape[1]):
            at = slice(p * wide, (p + 1) * wide)
            cb = conv[:, at]
            both = jnp.dot(cb, diag[layer, p], preferred_element_type=F32, precision=lax.Precision.HIGHEST)
            rgate = jax.nn.sigmoid(both[:, :wide])
            igate = jax.nn.sigmoid(both[:, wide:])
            loga = rgate * keep[:, at]
            decay = jnp.exp(loga)
            new = decay * hid[layer, :, at] + jnp.sqrt(-jnp.tanh(loga) * (1.0 + decay * decay)) * (igate * cb)
            hidden_out[layer, :, at] = new
            mix[layer, dp, :, at] = (new * gated[:, at]).astype(BF16)

    def share_and_emit(layer):
        own = mix.at[layer, dp]
        for k in range(1, ny):
            send(own, own, c1_s.at[layer, k], c1_r.at[layer, k], on_dp(partner(y, k, ny), c))
        for j in range(1, nc):
            send(own, own, c2_s.at[layer, 0, j], c2_r.at[layer, 0, j], on_dp(y, partner(c, j, nc)))
        loads["outw", layer].wait()
        if per_z == 1:
            emit(layer, dp)
        later = []
        for k in range(ny):
            yy = partner(y, k, ny)
            if k:
                theirs = mix.at[layer, yy * nc + c]
                arrived(theirs, c1_s.at[layer, k], c1_r.at[layer, k], on_dp(yy, c))
                for j in range(1, nc):
                    send(theirs, theirs, c2_s.at[layer, k, j], c2_r.at[layer, k, j], on_dp(y, partner(c, j, nc)))
                if per_z == 1:
                    emit(layer, yy * nc + c)
            for j in range(1, nc):
                cc = partner(c, j, nc)
                arrived(
                    mix.at[layer, yy * nc + cc], c2_s.at[layer, k, j], c2_r.at[layer, k, j], on_dp(y, cc)
                )
                if per_z == 1:
                    emit(layer, yy * nc + cc)
        if per_z != 1:
            for zz in range(nz):
                emit(layer, zz)

    def emit(layer, zz):
        block = mix[layer, pl.ds(zz * per_z, per_z)].reshape(per_z * chunk, chans)
        upd[layer, pl.ds(zz * nx, nx)] = (
            jnp.dot(block, wout[layer], preferred_element_type=F32).astype(BF16).reshape(nx, rows, cols)
        )
        for j in range(1, nx):
            xx = partner(x, j, nx)
            send(
                upd.at[layer, zz * nx + xx], x_in.at[layer, j, zz],
                d1_s.at[layer, j, zz], d1_r.at[layer, j, zz], on_tp(z, xx),
            )

    def reduce_stream(layer):
        total = None
        for k in list(range(1, nz)) + [0]:
            zz = partner(z, k, nz)
            both = upd[layer, zz * nx + x].astype(F32)
            for j in range(1, nx):
                arrived(
                    x_in.at[layer, j, zz], d1_s.at[layer, j, zz], d1_r.at[layer, j, zz], on_tp(z, partner(x, j, nx))
                )
                both = both + x_in[layer, j, zz].astype(F32)
            if k:
                z_send[layer, k] = both.astype(BF16)
                send(z_send.at[layer, k], z_in.at[layer, k], d2_s.at[layer, k], d2_r.at[layer, k], on_tp(zz, x))
            else:
                total = both
        for k in range(1, nz):
            arrived(z_in.at[layer, k], d2_s.at[layer, k], d2_r.at[layer, k], on_tp(partner(z, k, nz), x))
            total = total + z_in[layer, k].astype(F32)
        return (xg[layer, tp].astype(F32) + total).astype(BF16)

    gather_start(0)
    for layer in range(layers):
        load("hidden", layer, hidden_hbm, hid, load_sem.at[layer, 2])
        load("convpart", layer, convpart_hbm, convp, load_sem.at[layer, 3])
        load("outw", layer, outw_hbm, wout, load_sem.at[layer, 4])
        if layer:
            load("path", layer, path_hbm, wpath, load_sem.at[layer, 0])
            load("gate", layer, gate_hbm, wgate, load_sem.at[layer, 1])

    width = rmap.shape[2]
    row = lax.broadcasted_iota(jnp.int32, (width, 2 * width), 0)
    col = lax.broadcasted_iota(jnp.int32, (width, 2 * width), 1)
    place = [jnp.where(col == row + half * width, 1.0, 0.0).astype(F32) for half in range(2)]
    for layer in range(layers):
        loads["rmap", layer].wait()
        loads["imap", layer].wait()
        for p in range(diag.shape[1]):
            for half in range(2):
                for which, maps in enumerate((rmap, imap)):
                    diag[
                        layer, p, half * width : (half + 1) * width, which * 2 * width : (which + 1) * 2 * width
                    ] = jnp.dot(
                        maps[layer, 2 * p + half], place[half],
                        preferred_element_type=F32, precision=lax.Precision.HIGHEST,
                    )

    for layer in range(layers):
        gather_and_project(layer)
        recur(layer, reduce_rows(layer))
        share_and_emit(layer)
        new = reduce_stream(layer)
        if layer + 1 < layers:
            xg[layer + 1, tp] = new
            gather_start(layer + 1)
        else:
            stream_out[...] = new
    for copy in sends:
        copy.wait_send()


def per_device(
    grid,
    stream_in, hidden_state, window, norm_gain, path_weight, output_gate_weight,
    conv_taps, recur_map, input_map, decay_logit, out_weight,
):
    nz, nx, ny, nc = grid
    rows, cols = stream_in.shape
    layers, chunk, chans = hidden_state.shape
    tp, dp = nz * nx, ny * nc
    width = recur_map.shape[2]
    blocks = recur_map.shape[1]
    taps = conv_taps.shape[1]
    convpart = sum(window[:, :, j].astype(F32) * conv_taps[:, j][:, None, :] for j in range(taps - 1))
    wide = 2 * chans + LANES
    vm = pl.BlockSpec(memory_space=pltpu.VMEM)
    hbm = pl.BlockSpec(memory_space=pl.ANY)
    dma = pltpu.SemaphoreType.DMA
    stream_out, hidden_next, zpath = pl.pallas_call(
        functools.partial(step_kernel, (layers, nz, nx, ny, nc, cols * dp)),
        out_shape=(
            jax.ShapeDtypeStruct((rows, cols), BF16),
            jax.ShapeDtypeStruct((layers, chunk, chans), F32),
            jax.ShapeDtypeStruct((layers, chunk, chans), BF16),
        ),
        in_specs=[vm, hbm, hbm, vm, hbm, hbm, vm, hbm, hbm, vm, hbm],
        out_specs=(vm, vm, vm),
        scratch_shapes=[
            pltpu.VMEM((layers, tp, rows, cols), BF16),
            pltpu.VMEM((layers, dp, chunk, wide), BF16),
            pltpu.VMEM((layers, nc, ny, chunk, wide), BF16),
            pltpu.VMEM((layers, ny, chunk, wide), BF16),
            pltpu.VMEM((layers, ny, chunk, wide), BF16),
            pltpu.VMEM((layers, dp, chunk, chans), BF16),
            pltpu.VMEM((layers, tp, rows, cols), BF16),
            pltpu.VMEM((layers, nx, nz, rows, cols), BF16),
            pltpu.VMEM((layers, nz, rows, cols), BF16),
            pltpu.VMEM((layers, nz, rows, cols), BF16),
            pltpu.VMEM((layers, cols, chans), BF16),
            pltpu.VMEM((layers, cols, chans), BF16),
            pltpu.VMEM((layers, chans, cols), BF16),
            pltpu.VMEM((layers, chunk, chans), F32),
            pltpu.VMEM((layers, chunk, chans), F32),
            pltpu.VMEM((layers, blocks, width, width), F32),
            pltpu.VMEM((layers, blocks, width, width), F32),
            pltpu.VMEM((layers, blocks // 2, 2 * width, 4 * width), F32),
            dma((layers, 5)), dma((layers, 2)),
            dma((layers, nz)), dma((layers, nz)), dma((layers, nz, nx)), dma((layers, nz, nx)),
            dma((layers, nc, ny)), dma((layers, nc, ny)), dma((layers, ny)), dma((layers, ny)),
            dma((layers, ny)), dma((layers, ny)), dma((layers, ny, nc)), dma((layers, ny, nc)),
            dma((layers, nx, nz)), dma((layers, nx, nz)), dma((layers, nz)), dma((layers, nz)),
        ],
        compiler_params=pltpu.CompilerParams(
            collective_id=0, has_side_effects=True, vmem_limit_bytes=48 * 1024 * 1024
        ),
    )(
        stream_in, hidden_state, convpart, norm_gain, path_weight, output_gate_weight,
        conv_taps, recur_map, input_map, decay_logit, out_weight,
    )
    return stream_out, hidden_next, jnp.concatenate([window[:, :, 1:], zpath[:, :, None]], axis=2)


def physical(mesh):
    first = mesh.devices.flat[0]
    tp, dp = mesh.shape["tp"], mesh.shape["dp"]
    if getattr(first, "coords", None) is None:
        nx, nc = 2, 2
    else:
        nx = len({d.coords[0] for d in mesh.devices.flat})
        nc = len({d.core_on_chip for d in mesh.devices.flat})
    return tp // nx, nx, dp // nc, nc


def solution(mesh):
    placed = (
        P("tp", "dp"),
        P(None, "dp", "tp"),
        P(None, "dp", None, "tp"),
        P(None, "dp"),
        P(None, "dp", "tp"),
        P(None, "dp", "tp"),
        P(None, None, "tp"),
        P(None, "tp", None, None),
        P(None, "tp", None, None),
        P(None, "tp"),
        P(None, "tp", "dp"),
    )
    return jax.shard_map(
        functools.partial(per_device, physical(mesh)),
        mesh=mesh,
        in_specs=placed,
        out_specs=(P("tp", "dp"), P(None, "dp", "tp"), P(None, "dp", None, "tp")),
        check_vma=False,
    )
```

time: 274 us -> 85.1 us (0.31)
  waiting for transfers between devices: 178 us -> 0 us
  Pallas kernels: 0 us -> 72.3 us
  blocking collectives: 56.1 us -> 0 us
  matrix products: 14.2 us -> 0 us
  between operations: 14 us -> 0.68 us
  local copies, waits for them, and re-layouts: 2.29 us -> 9.75 us
  other arithmetic: 8.41 us -> 1.89 us
    reduce_scatter x3 -> x0, waiting for transfers between devices: 105 us -> none  [the longest x1 61.1 us: per_device(): lax.psum_scatter(update.astype(jnp.bfloat16), 'tp', scatter_dimension=0,...]
    psum x1 -> x0, waiting for transfers between devices: 72.8 us -> none  [per_device(): lax.psum(update.astype(jnp.bfloat16), 'tp').astype(jnp.float32)]
    pallas_call x0 -> x1, Pallas kernels: none -> 72.3 us  [per_device(): pl.pallas_call(functools.partial(step_kernel, (layers, nz, nx, ny, nc, co...]
    all_gather x3 -> x0, blocking collectives: 44.8 us -> none  [the longest x1 33.3 us: per_device(): whole_rows = lax.all_gather(stream, 'tp', axis=0, tiled=True)]
    dot_general x10 -> x0, matrix products: 14.2 us -> none  [the longest x2 4.94 us: recur_tail(): jnp.dot(lax.all_gather(mixed, 'dp', axis=0, tiled=True), out_w, preferred...]
    psum x2 -> x0, blocking collectives: 11.3 us -> none  [scaled(): sumsq = lax.psum(jnp.sum(rowsf * rowsf, axis=1), 'dp')]
    unnamed x16 -> x20, local copies, waits for them, and re-layouts: 0.04 us -> 8.9 us
  transfers between devices with their start and end apart: 4 -> 0, of which waited for: 4 -> 0; matrix products, arithmetic and copies ran while one was open for 1% -> 0% of each run, Pallas kernels for 0% -> 0%
where the time goes in v1:
time: 85.1 us; the launch traced here: 84.6 us
  Pallas kernels  72.3 us (85%)
  local copies, waits for them, and re-layouts  9.75 us (11%)
  other arithmetic  1.89 us (2%)
    pallas_call x1, Pallas kernels, per_device(): pl.pallas_call(functools.partial(step_kernel, (layers, nz, nx, ny, nc, co...  72.3 us
    unnamed x20, local copies, waits for them, and re-layouts  8.9 us

profile of v1, /device:TPU:0, one launch (start us, length us, event | category | flops | bytes accessed | tf_op | source)
XLA Modules:
  0.0 84.6 jit_solution(17273253498161516714)
XLA Ops:
  0.6 0.8 fusion.2
  1.5 1.1 %fusion.convpart_hbm = f32[2,64,512]{2,1,0:T(8,128)S(1)} fusion(f32[2,512]{1,0:T(2,128)S(1)} %get-tuple-element.12, bf16[2,64,3,512]{3,1,2,0:T(8,128)(2,1)} %param.13, f32[2,512]{1,0:T(2,128)S(1)} %get-tuple-element.13, f32[2,512]{1,0:T(2,128)S(1)} %bitcast.26), kind=kLoop, calls=%fused_computation.2 | loop fusion | flops 524288 | bytes 667648 | tf_op jit(solution)/shard_map/add | solution.py:317
  2.6 0.0 copy-start
  2.6 1.6 %copy-done = bf16[2,1024,512]{2,1,0:T(8,128)(2,1)S(1)} copy-done((bf16[2,1024,512]{2,1,0:T(8,128)(2,1)S(1)}, bf16[2,1024,512]{2,1,0:T(8,128)(2,1)}, u32[]{:S(2)}) %copy-start) | copy-done | bytes 2097176
  4.2 0.0 copy-start.1
  4.2 1.0 %copy-done.1 = f32[2,8,64,64]{3,2,1,0:T(8,128)S(1)} copy-done((f32[2,8,64,64]{3,2,1,0:T(8,128)S(1)}, f32[2,8,64,64]{3,2,1,0:T(8,128)}, u32[]{:S(2)}) %copy-start.1) | copy-done | bytes 262168
  5.3 0.0 copy-start.2
  5.3 1.0 %copy-done.2 = f32[2,8,64,64]{3,2,1,0:T(8,128)S(1)} copy-done((f32[2,8,64,64]{3,2,1,0:T(8,128)S(1)}, f32[2,8,64,64]{3,2,1,0:T(8,128)}, u32[]{:S(2)}) %copy-start.2) | copy-done | bytes 262168
  6.3 0.0 copy-start.3
  6.3 0.9 %copy-done.3 = f32[2,64,512]{2,1,0:T(8,128)S(1)} copy-done((f32[2,64,512]{2,1,0:T(8,128)S(1)}, f32[2,64,512]{2,1,0:T(8,128)}, u32[]{:S(2)}) %copy-start.3) | copy-done | bytes 262168
  7.2 0.0 copy-start.4
  7.2 0.8 copy-done.4
  8.1 0.0 copy-start.5
  8.1 0.7 copy-done.5
  8.8 0.0 copy-start.6
  8.8 0.7 copy-done.6
  9.5 0.0 copy-start.7
  9.5 0.7 copy-done.7
  10.2 0.0 slice-start
  10.2 72.3 %shard_map.130 = (bf16[32,1024]{1,0:T(8,128)(2,1)S(1)}, f32[2,64,512]{2,1,0:T(8,128)S(1)}, bf16[2,64,512]{2,1,0:T(8,128)(2,1)S(1)}) custom-call(bf16[32,1024]{1,0:T(8,128)(2,1)S(1)} %copy-done.4, f32[2,64,512]{2,1,0:T(8,128)S(1)} %copy-done.3, f32[2,64,512]{2,1,0:T(8,128)S(1)} %fusion.convpart_hbm, f32[2,1024]{1,0:T(2,128)S(1)} %copy-done.6, ...), custom_call_target="tpu_custom_call" | custom-call | tf_op jit(solution)/shard_map/pallas_call | solution.py:322
  82.5 0.0 slice-done
  82.5 0.8 pad_maximum_fusion
  83.3 0.6 copy.34
  83.9 0.7 copy.35
  (2 shorter events, 0.0 us)
Async XLA Ops:
  2.6 1.6 %copy-start = (bf16[2,1024,512]{2,1,0:T(8,128)(2,1)S(1)}, bf16[2,1024,512]{2,1,0:T(8,128)(2,1)}, u32[]{:S(2)}) copy-start(bf16[2,1024,512]{2,1,0:T(8,128)(2,1)} %path_hbm.1) | copy-start | bytes 6291460
  4.2 1.0 %copy-start.1 = (f32[2,8,64,64]{3,2,1,0:T(8,128)S(1)}, f32[2,8,64,64]{3,2,1,0:T(8,128)}, u32[]{:S(2)}) copy-start(f32[2,8,64,64]{3,2,1,0:T(8,128)} %rmap_hbm.1) | copy-start | bytes 786436
  5.3 1.0 %copy-start.2 = (f32[2,8,64,64]{3,2,1,0:T(8,128)S(1)}, f32[2,8,64,64]{3,2,1,0:T(8,128)}, u32[]{:S(2)}) copy-start(f32[2,8,64,64]{3,2,1,0:T(8,128)} %imap_hbm.1) | copy-start | bytes 786436
  6.3 0.9 %copy-start.3 = (f32[2,64,512]{2,1,0:T(8,128)S(1)}, f32[2,64,512]{2,1,0:T(8,128)}, u32[]{:S(2)}) copy-start(f32[2,64,512]{2,1,0:T(8,128)} %hidden_hbm.1) | copy-start | bytes 786436
  7.2 0.8 copy-start.4
  8.1 0.7 copy-start.5
  8.8 0.7 copy-start.6
  9.5 0.7 copy-start.7
  10.2 72.3 %slice-start = ((bf16[2,64,3,512]{3,1,2,0:T(8,128)(2,1)}), bf16[2,64,2,512]{3,1,2,0:T(8,128)(2,1)S(1)}, s32[]{:S(2)}) async-start(bf16[2,64,3,512]{3,1,2,0:T(8,128)(2,1)} %param.13), calls=%async_computation | async-start | bytes 524288 | tf_op jit(solution)/shard_map/slice | solution.py:363

commit v2 on v1

--- a/solution.py
+++ b/solution.py
@@ -39,11 +39,11 @@
 
 def step_kernel(
     sizes,
-    stream, hidden_hbm, convpart_hbm, gain, path_hbm, gate_hbm, taps, rmap_hbm, imap_hbm, logit, outw_hbm,
-    stream_out, hidden_out, zpath_out,
+    stream_hbm, hidden_hbm, win_hbm, gain_hbm, path_hbm, gate_hbm, taps_hbm, rmap_hbm, imap_hbm, logit_hbm, outw_hbm,
+    stream_out, hidden_out, window_out,
     xg, part, core_in, y_send, y_in, mix, upd, x_in, z_send, z_in,
-    wpath, wgate, wout, hid, convp, rmap, imap, diag,
-    load_sem, load_small, ag_s, ag_r, fw_s, fw_r, b1_s, b1_r, b2_s, b2_r,
+    wpath, wgate, wout, hid, convp, rmap, imap, diag, win, gain, taps, logit,
+    load_sem, load_small, load_once, ag_s, ag_r, fw_s, fw_r, b1_s, b1_r, b2_s, b2_r,
     c1_s, c1_r, c2_s, c2_r, d1_s, d1_r, d2_s, d2_r,
 ):
     layers, nz, nx, ny, nc, model = sizes
@@ -51,7 +51,7 @@
     dp = lax.axis_index("dp")
     z, x = tp // nx, tp % nx
     y, c = dp // nc, dp % nc
-    rows, cols = stream.shape
+    rows, cols = stream_out.shape
     chans = wpath.shape[2]
     per_z = mix.shape[1] // nz
     chunk = mix.shape[2]
@@ -78,22 +78,33 @@
     barrier = pltpu.get_barrier_semaphore()
     for peer in peers:
         pl.semaphore_signal(barrier, inc=1, device_id=peer, device_id_type=MESH)
-    xg[0, tp] = stream[...]
+    once = [
+        pltpu.make_async_copy(src, dst, load_once.at[at])
+        for at, (src, dst) in enumerate(
+            ((stream_hbm, xg.at[0, tp]), (gain_hbm, gain), (taps_hbm, taps), (logit_hbm, logit))
+        )
+    ]
+    for copy in once:
+        copy.start()
     load("path", 0, path_hbm, wpath, load_sem.at[0, 0])
     load("gate", 0, gate_hbm, wgate, load_sem.at[0, 1])
     for layer in range(layers):
         load("rmap", layer, rmap_hbm, rmap, load_small.at[layer, 0])
         load("imap", layer, imap_hbm, imap, load_small.at[layer, 1])
+    once[0].wait()
     pl.semaphore_wait(barrier, len(peers))
 
     sends = []
 
-    def send(src, dst, ssem, rsem, peer):
+    def send(src, dst, ssem, rsem, peer, cond=None):
         copy = pltpu.make_async_remote_copy(
             src_ref=src, dst_ref=dst, send_sem=ssem, recv_sem=rsem, device_id=peer, device_id_type=MESH
         )
-        copy.start()
-        sends.append(copy)
+        sends.append((copy, cond))
+        if cond is None:
+            copy.start()
+        else:
+            pl.when(cond)(copy.start)
 
     def arrived(dst, ssem, rsem, peer):
         pltpu.make_async_remote_copy(
@@ -102,11 +113,10 @@
 
     def gather_start(layer):
         own = xg.at[layer, tp]
-        source = stream if layer == 0 else own
         for k in range(1, nz):
-            send(source, own, ag_s.at[layer, k], ag_r.at[layer, k], on_tp(partner(z, k, nz), x))
+            send(own, own, ag_s.at[layer, k], ag_r.at[layer, z], on_tp(partner(z, k, nz), x))
         for j in range(1, nx):
-            send(source, own, fw_s.at[layer, 0, j], fw_r.at[layer, 0, j], on_tp(z, partner(x, j, nx)))
+            send(own, own, fw_s.at[layer, nz, j], fw_r.at[layer, z, j], on_tp(z, partner(x, j, nx)))
 
     def project(layer, zz):
         block = xg[layer, pl.ds(zz * nx, nx)].reshape(nx * rows, cols).astype(F32)
@@ -122,55 +132,60 @@
         )
         part[layer, here, :, 2 * chans :] = pack_col(square).reshape(*shape, LANES)
 
-    def gather_and_project(layer):
-        for k in range(nz):
-            zz = partner(z, k, nz)
-            if k:
-                own = xg.at[layer, zz * nx + x]
-                arrived(own, ag_s.at[layer, k], ag_r.at[layer, k], on_tp(zz, x))
-                for j in range(1, nx):
-                    send(own, own, fw_s.at[layer, k, j], fw_r.at[layer, k, j], on_tp(z, partner(x, j, nx)))
-            if k == 0:
+    def forward(layer, zz):
+        own = xg.at[layer, zz * nx + x]
+
+        def wait():
+            arrived(own, ag_s.at[layer, 0], ag_r.at[layer, zz], on_tp(partner(z, 1, nz), x))
+
+        pl.when(zz != z)(wait)
+        for j in range(1, nx):
+            send(
+                own, own, fw_s.at[layer, zz, j], fw_r.at[layer, zz, j], on_tp(z, partner(x, j, nx)), zz != z
+            )
+
+    def reduce_cores(layer, yy):
+        both = part[layer, yy * nc + c].astype(F32)
+        for j in range(1, nc):
+            arrived(
+                core_in.at[layer, j, yy], b1_s.at[layer, 0], b1_r.at[layer, j, yy], on_dp(y, partner(c, j, nc))
+            )
+            both = both + core_in[layer, j, yy].astype(F32)
+        return both
+
+    def gather_project_reduce(layer):
+        each = nz // ny
+        order = [
+            (ky, partner(y, ky, ny) * each + partner(z % each, kl, each))
+            for ky in list(range(1, ny)) + [0]
+            for kl in range(each)
+        ]
+        forward(layer, order[0][1])
+        for at, (ky, zz) in enumerate(order):
+            if at + 1 < nz:
+                forward(layer, order[at + 1][1])
+            if at == 0:
                 loads["path", layer].wait()
                 loads["gate", layer].wait()
-            else:
-                finish_block(layer, k - 1)
-        finish_block(layer, nz - 1)
-
-    def finish_block(layer, k):
-        zz = partner(z, k, nz)
-        for j in range(1, nx):
-            xx = partner(x, j, nx)
-            arrived(xg.at[layer, zz * nx + xx], fw_s.at[layer, k, j], fw_r.at[layer, k, j], on_tp(z, xx))
-        project(layer, zz)
-
-    def reduce_rows(layer):
-        order = list(range(1, ny)) + [0]
-        for k in order:
-            yy = partner(y, k, ny)
-            for j in range(1, nc):
-                cc = partner(c, j, nc)
-                send(
-                    part.at[layer, yy * nc + cc], core_in.at[layer, j, k],
-                    b1_s.at[layer, j, k], b1_r.at[layer, j, k], on_dp(y, cc),
-                )
-        total = None
-        for k in order:
-            yy = partner(y, k, ny)
-            both = part[layer, yy * nc + c].astype(F32)
-            extra = None
-            for j in range(1, nc):
-                arrived(
-                    core_in.at[layer, j, k], b1_s.at[layer, j, k], b1_r.at[layer, j, k],
-                    on_dp(y, partner(c, j, nc)),
-                )
-                both = both + core_in[layer, j, k].astype(F32)
-            if k:
-                y_send[layer, k, :, 0 : 2 * chans] = both[:, : 2 * chans].astype(BF16)
-                y_send[layer, k, :, 2 * chans :] = pack_col(unpack_col(both[:, 2 * chans :]))
-                send(y_send.at[layer, k], y_in.at[layer, k], b2_s.at[layer, k], b2_r.at[layer, k], on_dp(yy, c))
-            else:
-                total = both
+            for j in range(1, nx):
+                xx = partner(x, j, nx)
+                arrived(xg.at[layer, zz * nx + xx], fw_s.at[layer, nz, j], fw_r.at[layer, zz, j], on_tp(z, xx))
+            project(layer, zz)
+            for i in range(per_z):
+                d = zz * per_z + i
+                for j in range(1, nc):
+                    cc = partner(c, j, nc)
+                    send(
+                        part.at[layer, d], core_in.at[layer, j, d // nc],
+                        b1_s.at[layer, d], b1_r.at[layer, j, d // nc], on_dp(y, cc), d % nc == cc,
+                    )
+            if at % each == each - 1 and ky:
+                yy = partner(y, ky, ny)
+                both = reduce_cores(layer, yy)
+                y_send[layer, ky, :, 0 : 2 * chans] = both[:, : 2 * chans].astype(BF16)
+                y_send[layer, ky, :, 2 * chans :] = pack_col(unpack_col(both[:, 2 * chans :]))
+                send(y_send.at[layer, ky], y_in.at[layer, ky], b2_s.at[layer, ky], b2_r.at[layer, ky], on_dp(yy, c))
+        total = reduce_cores(layer, y)
         for k in range(1, ny):
             arrived(y_in.at[layer, k], b2_s.at[layer, k], b2_r.at[layer, k], on_dp(partner(y, k, ny), c))
             total = total + y_in[layer, k].astype(F32)
@@ -178,11 +193,10 @@
 
     def recur(layer, total):
         loads["hidden", layer].wait()
-        loads["convpart", layer].wait()
         scale = lax.rsqrt(unpack_col(total[:, 2 * chans :]) / model + EPS)
         zpath = (total[:, :chans] * scale).astype(BF16)
         zgate = (total[:, chans : 2 * chans] * scale).astype(BF16).astype(F32)
-        zpath_out[layer] = zpath
+        window_out[layer, window_out.shape[1] - 1] = zpath
         last = taps.shape[1] - 1
         conv = convp[layer] + zpath.astype(F32) * taps[layer, last : last + 1, :]
         keep = jax.nn.log_sigmoid(logit[layer : layer + 1, :]) * 8.0
@@ -243,29 +257,34 @@
             )
 
     def reduce_stream(layer):
-        total = None
-        for k in list(range(1, nz)) + [0]:
-            zz = partner(z, k, nz)
+        if per_z == 1:
+            order = [
+                partner(y, ky, ny) * nc + partner(c, kc, nc) for ky in range(ny) for kc in range(nc)
+            ]
+        else:
+            order = list(range(nz))
+        for k, zz in enumerate(order):
             both = upd[layer, zz * nx + x].astype(F32)
             for j in range(1, nx):
                 arrived(
                     x_in.at[layer, j, zz], d1_s.at[layer, j, zz], d1_r.at[layer, j, zz], on_tp(z, partner(x, j, nx))
                 )
                 both = both + x_in[layer, j, zz].astype(F32)
-            if k:
-                z_send[layer, k] = both.astype(BF16)
-                send(z_send.at[layer, k], z_in.at[layer, k], d2_s.at[layer, k], d2_r.at[layer, k], on_tp(zz, x))
-            else:
-                total = both
+            z_send[layer, zz] = both.astype(BF16)
+            send(
+                z_send.at[layer, zz], z_in.at[layer, z], d2_s.at[layer, zz], d2_r.at[layer, z], on_tp(zz, x), zz != z
+            )
+        total = xg[layer, tp].astype(F32) + z_send[layer, z].astype(F32)
         for k in range(1, nz):
-            arrived(z_in.at[layer, k], d2_s.at[layer, k], d2_r.at[layer, k], on_tp(partner(z, k, nz), x))
-            total = total + z_in[layer, k].astype(F32)
-        return (xg[layer, tp].astype(F32) + total).astype(BF16)
+            zz = partner(z, k, nz)
+            arrived(z_in.at[layer, zz], d2_s.at[layer, zz], d2_r.at[layer, zz], on_tp(zz, x))
+            total = total + z_in[layer, zz].astype(F32)
+        return total.astype(BF16)
 
     gather_start(0)
     for layer in range(layers):
         load("hidden", layer, hidden_hbm, hid, load_sem.at[layer, 2])
-        load("convpart", layer, convpart_hbm, convp, load_sem.at[layer, 3])
+        load("window", layer, win_hbm, win, load_sem.at[layer, 3])
         load("outw", layer, outw_hbm, wout, load_sem.at[layer, 4])
         if layer:
             load("path", layer, path_hbm, wpath, load_sem.at[layer, 0])
@@ -288,9 +307,17 @@
                         preferred_element_type=F32, precision=lax.Precision.HIGHEST,
                     )
 
+    for copy in once[1:]:
+        copy.wait()
     for layer in range(layers):
-        gather_and_project(layer)
-        recur(layer, reduce_rows(layer))
+        loads["window", layer].wait()
+        count = win.shape[1]
+        convp[layer] = sum(win[layer, j].astype(F32) * taps[layer, j : j + 1, :] for j in range(count))
+        for j in range(1, count):
+            window_out[layer, j - 1] = win[layer, j]
+
+    for layer in range(layers):
+        recur(layer, gather_project_reduce(layer))
         share_and_emit(layer)
         new = reduce_stream(layer)
         if layer + 1 < layers:
@@ -298,8 +325,11 @@
             gather_start(layer + 1)
         else:
             stream_out[...] = new
-    for copy in sends:
-        copy.wait_send()
+    for copy, cond in sends:
+        if cond is None:
+            copy.wait_send()
+        else:
+            pl.when(cond)(copy.wait_send)
 
 
 def per_device(
@@ -314,19 +344,18 @@
     width = recur_map.shape[2]
     blocks = recur_map.shape[1]
     taps = conv_taps.shape[1]
-    convpart = sum(window[:, :, j].astype(F32) * conv_taps[:, j][:, None, :] for j in range(taps - 1))
     wide = 2 * chans + LANES
     vm = pl.BlockSpec(memory_space=pltpu.VMEM)
-    hbm = pl.BlockSpec(memory_space=pl.ANY)
+    hbm = pl.BlockSpec(memory_space=pltpu.HBM)
     dma = pltpu.SemaphoreType.DMA
-    stream_out, hidden_next, zpath = pl.pallas_call(
+    stream_out, hidden_next, window_next = pl.pallas_call(
         functools.partial(step_kernel, (layers, nz, nx, ny, nc, cols * dp)),
         out_shape=(
             jax.ShapeDtypeStruct((rows, cols), BF16),
             jax.ShapeDtypeStruct((layers, chunk, chans), F32),
-            jax.ShapeDtypeStruct((layers, chunk, chans), BF16),
+            jax.ShapeDtypeStruct((layers, taps - 1, chunk, chans), BF16),
         ),
-        in_specs=[vm, hbm, hbm, vm, hbm, hbm, vm, hbm, hbm, vm, hbm],
+        in_specs=[hbm] * 11,
         out_specs=(vm, vm, vm),
         scratch_shapes=[
             pltpu.VMEM((layers, tp, rows, cols), BF16),
@@ -347,20 +376,24 @@
             pltpu.VMEM((layers, blocks, width, width), F32),
             pltpu.VMEM((layers, blocks, width, width), F32),
             pltpu.VMEM((layers, blocks // 2, 2 * width, 4 * width), F32),
-            dma((layers, 5)), dma((layers, 2)),
-            dma((layers, nz)), dma((layers, nz)), dma((layers, nz, nx)), dma((layers, nz, nx)),
-            dma((layers, nc, ny)), dma((layers, nc, ny)), dma((layers, ny)), dma((layers, ny)),
+            pltpu.VMEM((layers, taps - 1, chunk, chans), BF16),
+            pltpu.VMEM((layers, cols), F32),
+            pltpu.VMEM((layers, taps, chans), F32),
+            pltpu.VMEM((layers, chans), F32),
+            dma((layers, 5)), dma((layers, 2)), dma((4,)),
+            dma((layers, nz)), dma((layers, nz)), dma((layers, nz + 1, nx)), dma((layers, nz, nx)),
+            dma((layers, dp)), dma((layers, nc, ny)), dma((layers, ny)), dma((layers, ny)),
             dma((layers, ny)), dma((layers, ny)), dma((layers, ny, nc)), dma((layers, ny, nc)),
             dma((layers, nx, nz)), dma((layers, nx, nz)), dma((layers, nz)), dma((layers, nz)),
         ],
         compiler_params=pltpu.CompilerParams(
-            collective_id=0, has_side_effects=True, vmem_limit_bytes=48 * 1024 * 1024
+            collective_id=0, has_side_effects=True, vmem_limit_bytes=67043328
         ),
     )(
-        stream_in, hidden_state, convpart, norm_gain, path_weight, output_gate_weight,
+        stream_in, hidden_state, jnp.transpose(window, (0, 2, 1, 3)), norm_gain, path_weight, output_gate_weight,
         conv_taps, recur_map, input_map, decay_logit, out_weight,
     )
-    return stream_out, hidden_next, jnp.concatenate([window[:, :, 1:], zpath[:, :, None]], axis=2)
+    return stream_out, hidden_next, jnp.transpose(window_next, (0, 2, 1, 3))
 
 
 def physical(mesh):

time: 85.1 us -> 75.2 us (0.88)
  the two profiles are of different devices: /device:TPU:0 before, /device:TPU:5 now
where the time goes in v2:
time: 75.2 us; the launch traced here: 75 us
  Pallas kernels  69.4 us (92%)
  local copies, waits for them, and re-layouts  4.92 us (7%)
    pallas_call x1, Pallas kernels, per_device(): pl.pallas_call(functools.partial(step_kernel, (layers, nz, nx, ny, nc, co...  69.4 us
    unnamed x3, local copies, waits for them, and re-layouts  4.92 us

profile of v2, /device:TPU:5, one launch (start us, length us, event | category | flops | bytes accessed | tf_op | source)
XLA Modules:
  0.0 75.0 jit_solution(11316991982905603992)
XLA Ops:
  0.6 69.4 %shard_map.130 = (bf16[32,1024]{1,0:T(8,128)(2,1)}, f32[2,64,512]{2,1,0:T(8,128)}, bf16[2,3,64,512]{3,2,1,0:T(8,128)(2,1)}) custom-call(bf16[32,1024]{1,0:T(8,128)(2,1)} %stream_hbm.1, f32[2,64,512]{2,1,0:T(8,128)} %hidden_hbm.1, bf16[2,3,64,512]{3,2,1,0:T(8,128)(2,1)} %bitcast.2, f32[2,1024]{1,0:T(2,128)} %gain_hbm.1, bf16[2,1024,512]{2,1,0:T(8,128)(2,1)} %path_hbm.1, ...), custom_call_target="tpu_custom_call" | custom-call | tf_op jit(solution)/shard_map/pallas_call | solution.py:351
  70.0 1.5 %copy.17 = bf16[32,1024]{1,0:T(8,128)(2,1)} copy(bf16[32,1024]{1,0:T(8,128)(2,1)} %get-tuple-element.12) | data formatting | bytes 131072
  71.5 1.7 %copy.18 = f32[2,64,512]{2,1,0:T(8,128)} copy(f32[2,64,512]{2,1,0:T(8,128)} %get-tuple-element.13) | data formatting | bytes 524288
  73.2 1.8 %copy.19 = bf16[2,64,3,512]{3,1,2,0:T(8,128)(2,1)} copy(bf16[2,64,3,512]{3,1,2,0:T(8,128)(2,1)} %bitcast.3) | data formatting | bytes 786432
